TPU v7x, 128 devices: a whole 4x4x4 slice. The times are simulated.
128 devices in a mesh: sp: 16 (over z, y), tp: 8 (over x, core).
Axes of the slice: x: 4, y: 4, z: 4, core: 2. Of those that a mesh axis runs over, the one named last changes fastest.
Arguments:
- queries: bfloat16 [12288, 2048], P('sp', 'tp'), may hold values from -11 to 11
- key_rows: bfloat16 [12288, 2048], P('sp', 'tp'), may hold values from -4.5 to 4.5
- value_rows: bfloat16 [12288, 2048], P('sp', 'tp'), may hold values from -6 to 6
- log_forget: float32 [12288, 32], P('sp', 'tp'), may hold values from -1477.56 to 0, as said below
- stream_in: bfloat16 [12288, 2048], P('sp'), may hold values from -6 to 6
- out_weight: bfloat16 [2048, 2048], P('tp'), may hold values from -0.52734375 to 0.52734375
- mix_gain: float32 [2048], replicated, may hold values from 0.1 to 1.9
- mix_bias: float32 [2048], replicated, may hold values from -3 to 3
- gate_weight: bfloat16 [2048, 5632], P('sp', 'tp'), may hold values from -0.125 to 0.125
- up_weight: bfloat16 [2048, 5632], P('sp', 'tp'), may hold values from -0.125 to 0.125
- down_weight: bfloat16 [5632, 2048], P('tp', 'sp'), may hold values from -0.15917969 to 0.15917969
- ffn_gain: float32 [2048], replicated, may hold values from 0.1 to 1.9
- ffn_bias: float32 [2048], replicated, may hold values from -3 to 3
Outputs:
- layer_out: bfloat16 [12288, 2048], P(('sp', 'tp'))
Inputs may be any that keep to these rules, and one draw needn't show every extreme that they name: `log_forget`: each column never rises along the positions.
All inputs are finite; a program needn't handle non-finite values.
Results may differ from a plain program's by a relative error of at most 0.015.
Values may be sent and summed in bfloat16 or wider, within the bound.
A program may use at most 128 MiB of HBM per device.

v0:
```python
import jax
import jax.numpy as jnp
from jax import lax
from jax.sharding import PartitionSpec as P

ALPHA = 8.0**0.25
EPSILON = 1e-05


def laid_out(pieces, dim):
    lengths = list(pieces.shape[1:])
    lengths[dim] *= pieces.shape[0]
    return jnp.moveaxis(pieces, 0, dim).reshape(lengths)


def from_everyone(value, axis):
    copies = jnp.broadcast_to(value, (lax.axis_size(axis), *value.shape))
    return lax.all_to_all(copies, axis, split_axis=0, concat_axis=0, tiled=True)


def gathered_copies(value, axis, dim):
    return laid_out(from_everyone(value, axis), dim)


def in_one_piece(arrays, axis, dim, along):
    ends, at = ([], 0)
    for a in arrays[:-1]:
        at += a.shape[along]
        ends.append(at)
    both = jnp.concatenate(arrays, axis=along)
    return tuple(jnp.split(lax.all_gather(both, axis, axis=dim, tiled=True), ends, axis=along))


def in_blocks(value, dim, count):
    before, after = (value.shape[:dim], value.shape[dim + 1 :])
    return jnp.moveaxis(value.reshape(*before, count, -1, *after), dim, 0)


def sum_at_owner(value, axis, dim):
    pieces = in_blocks(value, dim, lax.axis_size(axis))
    arrived = lax.all_to_all(pieces, axis, split_axis=0, concat_axis=0, tiled=True)
    return arrived.astype(jnp.float32).sum(axis=0)


def layer_norm(matrix, norm_gain, norm_shift):
    centred = matrix - jnp.mean(matrix, axis=-1, keepdims=True)
    spread = jnp.mean(centred * centred, axis=-1, keepdims=True)
    return centred * lax.rsqrt(spread + EPSILON) * norm_gain + norm_shift


def attend(queries, key_rows, value_rows, log_forget):
    length, row_width = queries.shape
    head_count = log_forget.shape[1]
    head_dim = row_width // head_count
    score_scale = head_dim ** (-0.5)
    first_pos = lax.axis_index("sp") * length
    last_pos = first_pos + length
    query_heads = queries.reshape(length, head_count, head_dim)
    query_gates = log_forget.T
    query_pos = first_pos + jnp.arange(length, dtype=jnp.int32)
    gates_all = gathered_copies(log_forget, "sp", 0)
    initial = (
        jnp.full((head_count, length), -1e30, jnp.float32),
        jnp.zeros((head_count, length), jnp.float32),
        jnp.zeros((length, head_count, head_dim), jnp.float32),
    )
    running = initial
    key_piece, value_piece = in_one_piece((key_rows, value_rows), "sp", 0, 1)
    piece_len = key_piece.shape[0]
    shards = piece_len // length
    group_size = max(
        [
            count_try
            for count_try in range(1, shards + 1)
            if shards % count_try == 0 and count_try * length <= max(length, 512)
        ]
    )
    block_len = group_size * length
    blocks = piece_len // block_len
    key_blocks = key_piece.reshape(blocks, block_len, head_count, head_dim)
    value_blocks = value_piece.reshape(blocks, block_len, head_count, head_dim)
    gate_blocks = gates_all.reshape(blocks, block_len, head_count)
    block_starts = block_len * jnp.arange(blocks, dtype=jnp.int32)

    def one_block(running_state, packed):
        key_block, value_block, gate_block, block_start = packed

        def compute(state_in):
            highest, totals, weighted = state_in
            scores = (
                jnp.einsum(
                    "qhd,khd->hqk", query_heads, key_block, preferred_element_type=jnp.float32
                )
                * score_scale
            )
            scores = scores + query_gates[:, :, None] - gate_block.T[:, None, :]
            key_pos = block_start + jnp.arange(block_len, dtype=jnp.int32)
            allowed = (key_pos[None, :] <= query_pos[:, None])[None]
            masked = jnp.where(allowed, scores, -1e30)
            new_high = jnp.maximum(highest, jnp.max(masked, axis=2))
            weights = jnp.where(allowed, jnp.exp(masked - new_high[:, :, None]), 0.0)
            factor = jnp.exp(highest - new_high)
            totals = totals * factor + jnp.sum(weights, axis=2)
            weighted = weighted * factor.T[:, :, None] + jnp.einsum(
                "hqk,khd->qhd",
                weights.astype(jnp.bfloat16),
                value_block,
                preferred_element_type=jnp.float32,
            )
            return (new_high, totals, weighted)

        def keep_state(state_in):
            return state_in

        return (lax.cond(block_start < last_pos, compute, keep_state, running_state), None)

    running, unused = lax.scan(
        one_block, running, (key_blocks, value_blocks, gate_blocks, block_starts)
    )
    highest, totals, weighted = running
    return (weighted / totals.T[:, :, None]).reshape(length, row_width).astype(jnp.bfloat16)


def body(
    queries,
    key_rows,
    value_rows,
    log_forget,
    stream_in,
    out_weight,
    mix_gain,
    mix_bias,
    gate_weight,
    up_weight,
    down_weight,
    ffn_gain,
    ffn_bias,
):
    attended = attend(queries, key_rows, value_rows, log_forget)
    length = attended.shape[0]
    own_rows = length // lax.axis_size("tp")
    offset = lax.axis_index("tp") * own_rows
    summed = sum_at_owner(
        jnp.dot(attended, out_weight, preferred_element_type=jnp.float32).astype(jnp.bfloat16),
        "tp",
        0,
    )
    mix_out = lax.optimization_barrier(summed.astype(jnp.bfloat16)).astype(jnp.float32)
    stream_own = lax.dynamic_slice_in_dim(stream_in, offset, own_rows, 0)
    normed = layer_norm(
        ALPHA * stream_own.astype(jnp.float32) + mix_out, mix_gain, mix_bias
    ).astype(jnp.bfloat16)
    gathered = lax.all_gather(normed, "tp", axis=0, tiled=True)
    pieces = in_one_piece((gate_weight, up_weight), "sp", 0, 1)
    gate_part = jnp.dot(gathered, pieces[0], preferred_element_type=jnp.float32)
    up_part = jnp.dot(gathered, pieces[1], preferred_element_type=jnp.float32)
    hidden = (jax.nn.silu(gate_part) * up_part).astype(jnp.bfloat16)
    partial_terms = jnp.dot(
        hidden,
        lax.all_gather(down_weight, "sp", axis=1, tiled=True),
        preferred_element_type=jnp.float32,
    )
    lowered = lax.psum_scatter(
        partial_terms.astype(jnp.bfloat16), "tp", scatter_dimension=0, tiled=True
    ).astype(jnp.float32)
    lowered = lax.optimization_barrier(lowered.astype(jnp.bfloat16)).astype(jnp.float32)
    result = layer_norm(ALPHA * normed.astype(jnp.float32) + lowered, ffn_gain, ffn_bias)
    return result.astype(jnp.bfloat16)


def solution(mesh):
    placed = (
        P("sp", "tp"),
        P("sp", "tp"),
        P("sp", "tp"),
        P("sp", "tp"),
        P("sp", None),
        P("tp", None),
        P(),
        P(),
        P("sp", "tp"),
        P("sp", "tp"),
        P("tp", "sp"),
        P(),
        P(),
    )
    return jax.shard_map(
        body, mesh=mesh, in_specs=placed, out_specs=P(("sp", "tp"), None), check_vma=False
    )
```

profile of v0, /device:TPU:0, one launch (start us, length us, event | category | flops | bytes accessed | tf_op | source)
XLA Modules:
  0.0 604.3 jit_solution(4880820120093457124)
XLA Ops:
  6.5 2.2 pad_maximum_fusion
  8.8 1.8 pad_maximum_fusion.1
  10.6 1.4 broadcast_in_dim.56
  12.0 8.2 %all-to-all-start = ((f32[16,768,4]{1,2,0:T(4,128)}), f32[16,768,4]{1,2,0:T(4,128)S(1)}, u32[]{:S(2)}, u32[]{:S(2)}) async-start(f32[16,768,4]{1,2,0:T(4,128)} %broadcast_in_dim.56), calls=%async_computation | async-start | bytes 393216 | tf_op jit(solution)/shard_map/all_to_all | solution.py:18
  20.2 1.2 copy.18
  21.4 80.5 %all-gather.5.cloned.1.call-done = bf16[12288,512]{1,0:T(8,128)(2,1)} async-done(((bf16[768,512]{1,0:T(8,128)(2,1)}), bf16[12288,512]{1,0:T(8,128)(2,1)}) %all-gather.5.cloned.1.call-update) | async-done | bytes 12582928 | tf_op jit(solution)/shard_map/all_gather | solution.py:31
  101.9 10.1 %fusion.36 = (bf16[12288,256]{1,0:T(8,128)(2,1)}, bf16[12288,256]{1,0:T(8,128)(2,1)}) fusion(bf16[12288,512]{1,0:T(8,128)(2,1)} %all-gather.5.cloned.1.call-done), kind=kLoop, calls=%fused_computation.51 | loop fusion | bytes 25165824 | tf_op jit(solution)/shard_map/split | solution.py:31
  112.0 18.8 %reshape.82 = bf16[16,768,4,64]{3,2,1,0:T(4,128)(2,1)} reshape(bf16[12288,256]{1,0:T(8,128)(2,1)} %get-tuple-element.249) | data formatting | bytes 12582912 | tf_op jit(solution)/shard_map/reshape | solution.py:80
  130.8 18.1 %copy.20 = bf16[16,768,4,64]{1,3,2,0:T(8,128)(2,1)} copy(bf16[16,768,4,64]{3,2,1,0:T(4,128)(2,1)} %reshape.82) | data formatting | bytes 12582912
  148.9 18.8 %reshape.83 = bf16[16,768,4,64]{3,2,1,0:T(4,128)(2,1)} reshape(bf16[12288,256]{1,0:T(8,128)(2,1)} %get-tuple-element.248) | data formatting | bytes 12582912 | tf_op jit(solution)/shard_map/reshape | solution.py:81
  167.6 18.1 %copy.21 = bf16[16,768,4,64]{1,3,2,0:T(8,128)(2,1)} copy(bf16[16,768,4,64]{3,2,1,0:T(4,128)(2,1)} %reshape.83) | data formatting | bytes 12582912
  185.8 33.5 %while.15 = (s32[]{:T(128)}, f32[4,768]{1,0:T(4,128)S(1)}, f32[4,768]{1,0:T(4,128)S(1)}, f32[768,4,64]{0,2,1:T(8,128)S(1)}, s32[16]{0:T(128)S(1)}, /*index=5*/s3...) while((s32[]{:T(128)}, f32[4,768]{1,0:T(4,128)S(1)}, ...), condition=%wide.region_5.6_spmd.clone, body=%wide.region_0.5_spmd.clone.sunk | while | flops 649800192 | bytes 33738040 | solution.py:117
  187.1 13.1 %conditional.3 = ((f32[4,768]{1,0:T(4,128)S(1)}, f32[4,768]{1,0:T(4,128)S(1)}, f32[768,4,64]{0,2,1:T(8,128)S(1)})) conditional(s32[]{:T(128)} %convert_element_type.100, (f32[4,768]{1,0:T(4,128)S(1)}, f32[4,768]{1,0:T(4,128)S(1)}, f32[768,4,64]{0,2,1:T(8,128)S(1)}) %tuple.41, (s32[]{:T(128)}, s32[]{:T(128)}, bf16[16,768,4,64]{1,3,2,0:T(8,128)(2,1)}, ...), branch_computations={%region_1.1_spmd, %region_2.4_spmd} | conditional | flops 649800192 | bytes 33734700 | solution.py:115
  187.1 0.7 iota_add_fusion
  188.2 3.9 fusion.4
  192.0 4.6 fusion.11
  196.6 3.5 fusion.3
  219.4 2.7 convolution_convert_fusion.1
  222.1 4.6 all-to-all-start.1
  226.9 38.2 %all-to-all-done.1 = bf16[8,96,2048]{2,1,0:T(8,128)(2,1)} async-done(((bf16[8,96,2048]{2,1,0:T(8,128)(2,1)}), bf16[8,96,2048]{2,1,0:T(8,128)(2,1)}, u32[]{:S(2)}, u32[]{:S(2)}) %all-to-all-start.1) | async-done | bytes 3145760 | tf_op jit(solution)/shard_map/all_to_all | solution.py:41
  265.1 2.5 reduce_sum.59
  267.6 1.2 fusion.33
  268.8 1.3 multiply_reduce_fusion.1
  270.2 2.0 add_convert_fusion.1
  272.8 220.0 %all-gather.7.cloned.1.call-done = bf16[768,2048]{1,0:T(8,128)(2,1)} async-done(((bf16[96,2048]{1,0:T(8,128)(2,1)}), bf16[768,2048]{1,0:T(8,128)(2,1)}) %all-gather.7.cloned.1.call-update) | async-done | bytes 3145744 | tf_op jit(solution)/shard_map/all_gather | solution.py:153
  492.8 6.5 %fusion.27 = f32[768,704]{0,1:T(8,128)} fusion(bf16[768,2048]{1,0:T(8,128)(2,1)} %all-gather.7.cloned.1.call-done, bf16[2048,1408]{0,1:T(8,128)(2,1)} %all-gather.9.cloned.1.call-done), kind=kOutput, calls=%fused_computation.31 | convolution fusion | flops 2214592512 | bytes 8192000 | tf_op jit(solution)/shard_map/dot_general | solution.py:155
  499.3 46.2 %all-gather.11.cloned.1.call-done = bf16[704,2048]{1,0:T(8,128)(2,1)} async-done(((bf16[704,128]{1,0:T(8,128)(2,1)}), bf16[704,2048]{1,0:T(8,128)(2,1)}) %all-gather.11.cloned.1.call-update) | async-done | bytes 2883600 | tf_op jit(solution)/shard_map/all_gather | solution.py:160
  545.5 12.4 %convolution_convert_fusion = bf16[768,2048]{1,0:T(8,128)(2,1)} fusion(bf16[704,2048]{1,0:T(8,128)(2,1)} %all-gather.11.cloned.1.call-done, f32[768,704]{0,1:T(8,128)} %fusion.27, bf16[768,2048]{1,0:T(8,128)(2,1)} %all-gather.7.cloned.1.call-done, bf16[2048,1408]{0,1:T(8,128)(2,1)} %all-gather.9.cloned.1.call-done), kind=kOutput, calls=%fused_computation.27 | convolution fusion | flops 4434001920 | bytes 14221312 | tf_op jit(solution)/shard_map/dot_general | solution.py:158
  557.9 35.3 %reduce-scatter.2.cloned.1.call-done = bf16[96,2048]{1,0:T(8,128)(2,1)} async-done(((bf16[768,2048]{1,0:T(8,128)(2,1)}), bf16[96,2048]{1,0:T(8,128)(2,1)}) %reduce-scatter.2.cloned.1.call-update) | async-done | bytes 393232 | tf_op jit(solution)/shard_map/reduce_scatter | solution.py:163
  593.2 1.2 fusion.34
  594.4 1.3 multiply_reduce_fusion
  595.7 2.0 add_convert_fusion
  (87 shorter events, 11.2 us)
Async XLA Ops:
  6.5 212.9 %copy-start = (bf16[256,2048]{1,0:T(8,128)(2,1)S(1)}, bf16[256,2048]{1,0:T(8,128)(2,1)}, u32[]{:S(2)}) copy-start(bf16[256,2048]{1,0:T(8,128)(2,1)} %param.22) | copy-start | bytes 3145732
  6.5 95.4 %all-gather.5.cloned.1.call-start = ((), (), s32[]{:S(2)}) async-start(), calls=%async_computation.3 | async-start | bytes 13369344 | tf_op jit(solution)/shard_map/all_gather | solution.py:31
  8.8 264.1 %all-gather.9.cloned.1.call-start = ((), (), s32[]{:S(2)}) async-start(), calls=%async_computation.5 | async-start | bytes 6127616 | tf_op jit(solution)/shard_map/all_gather | solution.py:31
  12.0 173.7 %all-to-all-start = ((f32[16,768,4]{1,2,0:T(4,128)}), f32[16,768,4]{1,2,0:T(4,128)S(1)}, u32[]{:S(2)}, u32[]{:S(2)}) async-start(f32[16,768,4]{1,2,0:T(4,128)} %broadcast_in_dim.56), calls=%async_computation | async-start | bytes 393216 | tf_op jit(solution)/shard_map/all_to_all | solution.py:18
  167.6 18.2 %copy-start.2 = (f32[768,4]{0,1:T(4,128)S(1)}, f32[768,4]{0,1:T(4,128)}, u32[]{:S(2)}) copy-start(f32[768,4]{0,1:T(4,128)} %param.20) | copy-start | bytes 36868
  222.1 48.0 %copy-start.3 = (f32[2048]{0:T(1024)S(1)}, f32[2048]{0:T(1024)}, u32[]{:S(2)}) copy-start(f32[2048]{0:T(1024)} %param.24) | copy-start | bytes 24580
  222.1 48.0 %copy-start.4 = (f32[2048]{0:T(1024)S(1)}, f32[2048]{0:T(1024)}, u32[]{:S(2)}) copy-start(f32[2048]{0:T(1024)} %param.23) | copy-start | bytes 24580
  222.1 43.0 %all-to-all-start.1 = ((bf16[8,96,2048]{2,1,0:T(8,128)(2,1)}), bf16[8,96,2048]{2,1,0:T(8,128)(2,1)}, u32[]{:S(2)}, u32[]{:S(2)}) async-start(bf16[8,96,2048]{2,1,0:T(8,128)(2,1)} %bitcast.45), calls=%async_computation.1 | async-start | bytes 6291456 | tf_op jit(solution)/shard_map/all_to_all | solution.py:41
  226.7 266.1 %all-gather.7.cloned.1.call-start = ((), (), s32[]{:S(2)}) async-start(), calls=%async_computation.4 | async-start | bytes 3538944 | tf_op jit(solution)/shard_map/all_gather | solution.py:153
  272.2 273.3 %all-gather.11.cloned.1.call-start = ((), (), s32[]{:S(2)}) async-start(), calls=%async_computation.6 | async-start | bytes 3063808 | tf_op jit(solution)/shard_map/all_gather | solution.py:160
  272.8 320.4 %reduce-scatter.2.cloned.1.call-start = ((), (), s32[]{:S(2)}) async-start(), calls=%async_computation.7 | async-start | bytes 3538944 | tf_op jit(solution)/shard_map/reduce_scatter | solution.py:163
  499.3 93.9 %copy-start.1 = (bf16[96,2048]{1,0:T(8,128)(2,1)S(1)}, bf16[96,2048]{1,0:T(8,128)(2,1)}, u32[]{:S(2)}) copy-start(bf16[96,2048]{1,0:T(8,128)(2,1)} %add_convert_fusion.1) | copy-start | bytes 1179652
  499.3 96.4 %copy-start.5 = (f32[2048]{0:T(1024)S(1)}, f32[2048]{0:T(1024)}, u32[]{:S(2)}) copy-start(f32[2048]{0:T(1024)} %param.29) | copy-start | bytes 24580
  499.3 96.4 %copy-start.6 = (f32[2048]{0:T(1024)S(1)}, f32[2048]{0:T(1024)}, u32[]{:S(2)}) copy-start(f32[2048]{0:T(1024)} %param.28) | copy-start | bytes 24580
Sparse Core Ops, SparseCore 0:
  9.5 92.3 all-gather.4
  104.0 64.0 all-gather.8
  272.3 220.4 all-gather.6
  494.8 50.6 all-gather.10
  558.0 35.0 reduce-scatter.1
where the time goes:
time: 608 us; the launch traced here: 604 us
  waiting for transfers between devices  421 us (69%)
  local copies, waits for them, and re-layouts  95.9 us (16%)
  matrix products  30.1 us (5%)
  other arithmetic  20.1 us (3%)
  between operations  13.3 us (2%)
  starting transfers between devices  13.1 us (2%)
  loops' own time  11.1 us (2%)
    all_gather x1, waiting for transfers between devices, body(): gathered = lax.all_gather(normed, 'tp', axis=0, tiled=True)  220 us
    all_gather x2, waiting for transfers between devices, in_one_piece(): lax.all_gather(both, axis, axis=dim, tiled=True)  80.5 us
    all_gather x1, waiting for transfers between devices, body(): lax.all_gather(down_weight, 'sp', axis=1, tiled=True)  46.2 us
    all_to_all x1, waiting for transfers between devices, sum_at_owner(): lax.all_to_all(pieces, axis, split_axis=0, concat_axis=0, tiled=True)  38.2 us
    unnamed x17, local copies, waits for them, and re-layouts  37.4 us
    reduce_scatter x1, waiting for transfers between devices, body(): lax.psum_scatter(partial_terms.astype(jnp.bfloat16), 'tp', scatter_dimens...  35.3 us
    reshape x1, local copies, waits for them, and re-layouts, attend(): key_blocks = key_piece.reshape(blocks, block_len, head_count, head_dim)  18.8 us
    reshape x1, local copies, waits for them, and re-layouts, attend(): value_blocks = value_piece.reshape(blocks, block_len, head_count, head_dim)  18.8 us
  transfers between devices with their start and end apart: 7, of which 5 were waited for; matrix products, arithmetic and copies ran while one was open for 21% of the time, Pallas kernels for 0%

commit v1 on v0

--- a/solution.py
+++ b/solution.py
@@ -150,7 +150,9 @@
     normed = layer_norm(
         ALPHA * stream_own.astype(jnp.float32) + mix_out, mix_gain, mix_bias
     ).astype(jnp.bfloat16)
-    gathered = lax.all_gather(normed, "tp", axis=0, tiled=True)
+    gathered = jnp.concatenate(
+        lax.all_to_all(jnp.stack([normed] * lax.axis_size("tp")), "tp", 0, 0), axis=0
+    )
     pieces = in_one_piece((gate_weight, up_weight), "sp", 0, 1)
     gate_part = jnp.dot(gathered, pieces[0], preferred_element_type=jnp.float32)
     up_part = jnp.dot(gathered, pieces[1], preferred_element_type=jnp.float32)

time: 608 us -> 579 us (0.952)
  waiting for transfers between devices: 421 us -> 386 us
    all_gather x1 -> x0, waiting for transfers between devices: 220 us -> none  [body(): gathered = lax.all_gather(normed, 'tp', axis=0, tiled=True)]
    all_gather x1, waiting for transfers between devices: 46.2 us -> 152 us  [body(): lax.all_gather(down_weight, 'sp', axis=1, tiled=True)]
    reduce_scatter x1, waiting for transfers between devices: 35.3 us -> 76.4 us  [body(): lax.psum_scatter(partial_terms.astype(jnp.bfloat16), 'tp', scatter_dimens...]
    all_to_all x0 -> x1, waiting for transfers between devices: none -> 38.3 us  [body(): lax.all_to_all(jnp.stack([normed] * lax.axis_size('tp')), 'tp', 0, 0)]
    unnamed x17 -> x15, local copies, waits for them, and re-layouts: 37.4 us -> 37.4 us
  transfers between devices with their start and end apart: 7 -> 7, of which waited for: 5 -> 5; matrix products, arithmetic and copies ran while one was open for 21% -> 22% of each run, Pallas kernels for 0% -> 0%
where the time goes in v1:
time: 579 us; the launch traced here: 575 us
  waiting for transfers between devices  386 us (67%)
  local copies, waits for them, and re-layouts  98.4 us (17%)
  matrix products  30.1 us (5%)
  other arithmetic  19.3 us (3%)
  starting transfers between devices  17.5 us (3%)
  between operations  13.3 us (2%)
  loops' own time  10.9 us (2%)
    all_gather x1, waiting for transfers between devices, body(): lax.all_gather(down_weight, 'sp', axis=1, tiled=True)  152 us
    all_gather x2, waiting for transfers between devices, in_one_piece(): lax.all_gather(both, axis, axis=dim, tiled=True)  80.5 us
    reduce_scatter x1, waiting for transfers between devices, body(): lax.psum_scatter(partial_terms.astype(jnp.bfloat16), 'tp', scatter_dimens...  76.4 us
    all_to_all x1, waiting for transfers between devices, body(): lax.all_to_all(jnp.stack([normed] * lax.axis_size('tp')), 'tp', 0, 0)  38.3 us
    all_to_all x1, waiting for transfers between devices, sum_at_owner(): lax.all_to_all(pieces, axis, split_axis=0, concat_axis=0, tiled=True)  37.7 us
    unnamed x15, local copies, waits for them, and re-layouts  37.4 us
    reshape x1, local copies, waits for them, and re-layouts, attend(): value_blocks = value_piece.reshape(blocks, block_len, head_count, head_dim)  18.8 us
    reshape x1, local copies, waits for them, and re-layouts, attend(): key_blocks = key_piece.reshape(blocks, block_len, head_count, head_dim)  18.8 us
  transfers between devices with their start and end apart: 7, of which 5 were waited for; matrix products, arithmetic and copies ran while one was open for 22% of the time, Pallas kernels for 0%

profile of v1, /device:TPU:0, one launch (start us, length us, event | category | flops | bytes accessed | tf_op | source)
XLA Modules:
  0.0 575.3 jit_solution(741586966160169847)
XLA Ops:
  6.5 2.2 pad_maximum_fusion
  8.8 1.8 pad_maximum_fusion.1
  10.6 1.4 broadcast_in_dim.56
  12.0 8.2 %all-to-all-start = ((f32[16,768,4]{1,2,0:T(4,128)}), f32[16,768,4]{1,2,0:T(4,128)S(1)}, u32[]{:S(2)}, u32[]{:S(2)}) async-start(f32[16,768,4]{1,2,0:T(4,128)} %broadcast_in_dim.56), calls=%async_computation | async-start | bytes 393216 | tf_op jit(solution)/shard_map/all_to_all | solution.py:18
  21.4 80.5 %all-gather.4.cloned.1.call-done = bf16[12288,512]{1,0:T(8,128)(2,1)} async-done(((bf16[768,512]{1,0:T(8,128)(2,1)}), bf16[12288,512]{1,0:T(8,128)(2,1)}) %all-gather.4.cloned.1.call-update) | async-done | bytes 12582928 | tf_op jit(solution)/shard_map/all_gather | solution.py:31
  101.9 10.1 %fusion.36 = (bf16[12288,256]{1,0:T(8,128)(2,1)}, bf16[12288,256]{1,0:T(8,128)(2,1)}) fusion(bf16[12288,512]{1,0:T(8,128)(2,1)} %all-gather.4.cloned.1.call-done), kind=kLoop, calls=%fused_computation.51 | loop fusion | bytes 25165824 | tf_op jit(solution)/shard_map/split | solution.py:31
  112.0 18.8 %reshape.88 = bf16[16,768,4,64]{3,2,1,0:T(4,128)(2,1)} reshape(bf16[12288,256]{1,0:T(8,128)(2,1)} %get-tuple-element.249) | data formatting | bytes 12582912 | tf_op jit(solution)/shard_map/reshape | solution.py:80
  130.8 18.1 %copy.20 = bf16[16,768,4,64]{1,3,2,0:T(8,128)(2,1)} copy(bf16[16,768,4,64]{3,2,1,0:T(4,128)(2,1)} %reshape.88) | data formatting | bytes 12582912
  148.9 18.8 %reshape.89 = bf16[16,768,4,64]{3,2,1,0:T(4,128)(2,1)} reshape(bf16[12288,256]{1,0:T(8,128)(2,1)} %get-tuple-element.248) | data formatting | bytes 12582912 | tf_op jit(solution)/shard_map/reshape | solution.py:81
  167.7 18.1 %copy.21 = bf16[16,768,4,64]{1,3,2,0:T(8,128)(2,1)} copy(bf16[16,768,4,64]{3,2,1,0:T(4,128)(2,1)} %reshape.89) | data formatting | bytes 12582912
  185.8 33.7 %while.15 = (s32[]{:T(128)}, f32[4,768]{1,0:T(4,128)S(1)}, f32[4,768]{1,0:T(4,128)S(1)}, f32[768,4,64]{0,2,1:T(8,128)S(1)}, s32[16]{0:T(128)S(1)}, /*index=5*/s3...) while((s32[]{:T(128)}, f32[4,768]{1,0:T(4,128)S(1)}, ...), condition=%wide.region_5.6_spmd.clone, body=%wide.region_0.5_spmd.clone.sunk | while | flops 649800192 | bytes 33738040 | solution.py:117
  187.1 13.1 %conditional.3 = ((f32[4,768]{1,0:T(4,128)S(1)}, f32[4,768]{1,0:T(4,128)S(1)}, f32[768,4,64]{0,2,1:T(8,128)S(1)})) conditional(s32[]{:T(128)} %convert_element_type.100, (f32[4,768]{1,0:T(4,128)S(1)}, f32[4,768]{1,0:T(4,128)S(1)}, f32[768,4,64]{0,2,1:T(8,128)S(1)}) %tuple.41, (s32[]{:T(128)}, s32[]{:T(128)}, bf16[16,768,4,64]{1,3,2,0:T(8,128)(2,1)}, ...), branch_computations={%region_1.1_spmd, %region_2.4_spmd} | conditional | flops 649800192 | bytes 33734700 | solution.py:115
  188.2 3.9 fusion.4
  192.1 4.6 fusion.11
  196.7 3.5 fusion.3
  219.6 2.7 convolution_convert_fusion.1
  222.3 4.6 all-to-all-start.1
  227.6 37.7 %all-to-all-done.1 = bf16[8,96,2048]{2,1,0:T(8,128)(2,1)} async-done(((bf16[8,96,2048]{2,1,0:T(8,128)(2,1)}), bf16[8,96,2048]{2,1,0:T(8,128)(2,1)}, u32[]{:S(2)}, u32[]{:S(2)}) %all-to-all-start.1) | async-done | bytes 3145760 | tf_op jit(solution)/shard_map/all_to_all | solution.py:41
  265.3 2.5 reduce_sum.59
  267.8 1.2 fusion.33
  269.0 1.3 multiply_reduce_fusion.1
  270.4 1.2 add_convert_fusion.1
  271.6 2.1 stack.2
  273.7 4.4 all-to-all-start.2
  278.2 38.3 %all-to-all-done.2 = bf16[8,96,2048]{2,1,0:T(8,128)(2,1)} async-done(((bf16[8,96,2048]{2,1,0:T(8,128)(2,1)}), bf16[8,96,2048]{2,1,0:T(8,128)(2,1)}, u32[]{:S(2)}, u32[]{:S(2)}) %all-to-all-start.2) | async-done | bytes 3145760 | tf_op jit(solution)/shard_map/all_to_all | solution.py:154
  316.6 6.6 %fusion.27 = f32[768,704]{0,1:T(8,128)} fusion(bf16[768,2048]{1,0:T(8,128)(2,1)} %bitcast.12, bf16[2048,1408]{0,1:T(8,128)(2,1)} %all-gather.6.cloned.1.call-done), kind=kOutput, calls=%fused_computation.31 | convolution fusion | flops 2214592512 | bytes 8192000 | tf_op jit(solution)/shard_map/dot_general | solution.py:157
  323.1 152.3 %all-gather.8.cloned.1.call-done = bf16[704,2048]{1,0:T(8,128)(2,1)} async-done(((bf16[704,128]{1,0:T(8,128)(2,1)}), bf16[704,2048]{1,0:T(8,128)(2,1)}) %all-gather.8.cloned.1.call-update) | async-done | bytes 2883600 | tf_op jit(solution)/shard_map/all_gather | solution.py:162
  475.4 12.4 %convolution_convert_fusion = bf16[768,2048]{1,0:T(8,128)(2,1)} fusion(bf16[704,2048]{1,0:T(8,128)(2,1)} %all-gather.8.cloned.1.call-done, f32[768,704]{0,1:T(8,128)} %fusion.27, bf16[768,2048]{1,0:T(8,128)(2,1)} %bitcast.12, bf16[2048,1408]{0,1:T(8,128)(2,1)} %all-gather.6.cloned.1.call-done), kind=kOutput, calls=%fused_computation.27 | convolution fusion | flops 4434001920 | bytes 14221312 | tf_op jit(solution)/shard_map/dot_general | solution.py:160
  487.9 76.4 %reduce-scatter.2.cloned.1.call-done = bf16[96,2048]{1,0:T(8,128)(2,1)} async-done(((bf16[768,2048]{1,0:T(8,128)(2,1)}), bf16[96,2048]{1,0:T(8,128)(2,1)}) %reduce-scatter.2.cloned.1.call-update) | async-done | bytes 393232 | tf_op jit(solution)/shard_map/reduce_scatter | solution.py:165
  564.3 1.2 fusion.34
  565.5 1.3 multiply_reduce_fusion
  566.8 2.0 add_convert_fusion
  (85 shorter events, 13.3 us)
Async XLA Ops:
  6.5 213.1 %copy-start = (bf16[256,2048]{1,0:T(8,128)(2,1)S(1)}, bf16[256,2048]{1,0:T(8,128)(2,1)}, u32[]{:S(2)}) copy-start(bf16[256,2048]{1,0:T(8,128)(2,1)} %param.22) | copy-start | bytes 3145732
  6.5 95.4 %all-gather.4.cloned.1.call-start = ((), (), s32[]{:S(2)}) async-start(), calls=%async_computation.4 | async-start | bytes 13369344 | tf_op jit(solution)/shard_map/all_gather | solution.py:31
  8.8 269.4 %all-gather.6.cloned.1.call-start = ((), (), s32[]{:S(2)}) async-start(), calls=%async_computation.5 | async-start | bytes 6127616 | tf_op jit(solution)/shard_map/all_gather | solution.py:31
  12.0 173.7 %all-to-all-start = ((f32[16,768,4]{1,2,0:T(4,128)}), f32[16,768,4]{1,2,0:T(4,128)S(1)}, u32[]{:S(2)}, u32[]{:S(2)}) async-start(f32[16,768,4]{1,2,0:T(4,128)} %broadcast_in_dim.56), calls=%async_computation | async-start | bytes 393216 | tf_op jit(solution)/shard_map/all_to_all | solution.py:18
  167.7 18.2 %copy-start.1 = (f32[768,4]{0,1:T(4,128)S(1)}, f32[768,4]{0,1:T(4,128)}, u32[]{:S(2)}) copy-start(f32[768,4]{0,1:T(4,128)} %param.20) | copy-start | bytes 36868
  222.3 48.0 %copy-start.2 = (f32[2048]{0:T(1024)S(1)}, f32[2048]{0:T(1024)}, u32[]{:S(2)}) copy-start(f32[2048]{0:T(1024)} %param.24) | copy-start | bytes 24580
  222.3 48.0 %copy-start.3 = (f32[2048]{0:T(1024)S(1)}, f32[2048]{0:T(1024)}, u32[]{:S(2)}) copy-start(f32[2048]{0:T(1024)} %param.23) | copy-start | bytes 24580
  222.3 43.0 %all-to-all-start.1 = ((bf16[8,96,2048]{2,1,0:T(8,128)(2,1)}), bf16[8,96,2048]{2,1,0:T(8,128)(2,1)}, u32[]{:S(2)}, u32[]{:S(2)}) async-start(bf16[8,96,2048]{2,1,0:T(8,128)(2,1)} %bitcast.46), calls=%async_computation.1 | async-start | bytes 6291456 | tf_op jit(solution)/shard_map/all_to_all | solution.py:41
  226.9 248.5 %all-gather.8.cloned.1.call-start = ((), (), s32[]{:S(2)}) async-start(), calls=%async_computation.6 | async-start | bytes 3063808 | tf_op jit(solution)/shard_map/all_gather | solution.py:162
  273.7 42.9 %all-to-all-start.2 = ((bf16[8,96,2048]{2,1,0:T(8,128)(2,1)}), bf16[8,96,2048]{2,1,0:T(8,128)(2,1)}, u32[]{:S(2)}, u32[]{:S(2)}) async-start(bf16[8,96,2048]{2,1,0:T(8,128)(2,1)} %stack.2), calls=%async_computation.2 | async-start | bytes 6291456 | tf_op jit(solution)/shard_map/all_to_all | solution.py:154
  278.1 286.1 %reduce-scatter.2.cloned.1.call-start = ((), (), s32[]{:S(2)}) async-start(), calls=%async_computation.7 | async-start | bytes 3538944 | tf_op jit(solution)/shard_map/reduce_scatter | solution.py:165
  323.1 243.7 %copy-start.4 = (f32[2048]{0:T(1024)S(1)}, f32[2048]{0:T(1024)}, u32[]{:S(2)}) copy-start(f32[2048]{0:T(1024)} %param.29) | copy-start | bytes 24580
  323.1 243.7 %copy-start.5 = (f32[2048]{0:T(1024)S(1)}, f32[2048]{0:T(1024)}, u32[]{:S(2)}) copy-start(f32[2048]{0:T(1024)} %param.28) | copy-start | bytes 24580
Sparse Core Ops, SparseCore 0:
  9.5 92.3 all-gather.3
  104.0 64.0 all-gather.5
  229.8 245.5 all-gather.7
  488.0 76.1 reduce-scatter.1
